TPU v7x, 768 devices: a whole 4x8x12 slice. The times are simulated.
768 devices in a mesh: fs: 96 (over z, y), tp: 8 (over x, core).
Axes of the slice: x: 4, y: 8, z: 12, core: 2. Of those that a mesh axis runs over, the one named last changes fastest.
Arguments:
- cotangent: bfloat16 [61440, 1024], P('fs', 'tp'), may hold values from -6 to 6
- inputs: bfloat16 [61440, 1024], P('fs', 'tp'), may hold values from -6 to 6
- pre_act: bfloat16 [61440, 2112], P('fs'), may hold values from -20 to 20
- w_up: bfloat16 [2112, 1024], P('fs', 'tp'), may hold values from -0.1875 to 0.1875
- w_down: bfloat16 [2112, 1024], P('fs', 'tp'), may hold values from -0.125 to 0.125
Outputs:
- grad_input: bfloat16 [61440, 1024], P('fs', 'tp')
- grad_up: float32 [2112, 1024], P('fs', 'tp')
All inputs are finite; a program needn't handle non-finite values.
Results may differ from a plain program's by a relative error of at most 0.0049.
Values may be sent and summed in bfloat16 or wider, within the bound.
A program may use at most 64 MiB of HBM per device.

v0:
```python
import jax
import jax.numpy as jnp
from jax import lax
from jax.sharding import Mesh
from jax.sharding import PartitionSpec as P

FS = ("fs_0", "fs_1")
TP = ("tp_0", "tp_1")


def cut_rows(length, count):
    unit = 8 if length >= 8 * count else 1
    return [length // unit * k // count * unit for k in range(1, count)]


def gather_in_order(array, axes, order):
    parts = array[None]
    for k in order:
        parts = lax.all_gather(parts, axes[k], axis=0, tiled=True)
    held = [lax.axis_size(axes[k]) for k in reversed(order)]
    parts = parts.reshape(*held, *array.shape)
    turned = sorted(range(len(order)), key=lambda place: order[len(order) - 1 - place])
    return parts.transpose(*turned, *range(len(order), parts.ndim)).reshape(-1, *array.shape)


def in_order(parts, dim):
    parts = jnp.moveaxis(parts, 0, dim)
    shape = parts.shape
    return parts.reshape(*shape[:dim], shape[dim] * shape[dim + 1], *shape[dim + 2 :])


def gather_all_axes(array, axes, dim):
    widest = max(range(max(1, array.ndim - 1)), key=lambda d: array.shape[d])
    count, done = (len(axes), [])
    for first, slab in enumerate(
        jnp.split(array, cut_rows(array.shape[widest], count), axis=widest)
    ):
        if slab.size:
            order = [(first - k) % count for k in range(count)]
            done.append(gather_in_order(slab, axes, order))
    return in_order(jnp.concatenate(done, axis=widest + 1), dim)


def copy_for_each(array, axis):
    copies = jnp.broadcast_to(array, (lax.axis_size(axis), *array.shape))
    return lax.all_to_all(copies, axis, split_axis=0, concat_axis=0, tiled=True)


def collect(array, axis, dim):
    return in_order(copy_for_each(array, axis), dim)


def whole_of(array, axes, order, dim):
    return in_order(gather_in_order(array, axes, order), dim)


def sum_in_order(parts, axes, order):
    shape = [lax.axis_size(a) for a in axes]
    parts = parts.reshape(*shape, *parts.shape[1:])
    parts = parts.transpose(*order, *range(len(axes), parts.ndim))
    parts = parts.reshape(-1, *parts.shape[len(axes) :])
    for k in order:
        parts = lax.psum_scatter(parts, axes[k], scatter_dimension=0, tiled=True)
    return parts[0]


def cut_along(array, dim, length):
    shape = array.shape
    parts = array.reshape(*shape[:dim], length, shape[dim] // length, *shape[dim + 1 :])
    return jnp.moveaxis(parts, dim, 0)


def sum_by_axis(array, axes, order, dim):
    length = lax.axis_size(axes)
    return sum_in_order(cut_along(array, dim, length), axes, order)


def times_rows(left, piece):
    return lax.dot_general(
        left, piece, (((1,), (1,)), ((), ())), preferred_element_type=jnp.float32
    )


def local(cotangent, inputs, pre_act, w_up, w_down):
    row_count = cotangent.shape[0]
    token_total = row_count * lax.axis_size(FS)
    full_cotangent = gather_all_axes(cotangent, TP, 1)
    down_whole = collect(w_down, TP, 1)
    grad_hidden = times_rows(full_cotangent, lax.all_gather(down_whole, FS, axis=0, tiled=True))
    grad_pre = (2.0 * grad_hidden * jnp.maximum(pre_act.astype(jnp.float32), 0.0)).astype(
        jnp.bfloat16
    )
    columns = grad_pre
    grad_input = jnp.dot(columns, whole_of(w_up, FS, (0, 1), 0), preferred_element_type=jnp.float32)
    columns = grad_pre
    grad_share = sum_by_axis(
        lax.dot_general(
            columns, inputs, (((0,), (0,)), ((), ())), preferred_element_type=jnp.float32
        ),
        FS,
        (1, 0),
        0,
    )
    grad_up = grad_share / jnp.sqrt(jnp.float32(token_total))
    return (grad_input.astype(jnp.bfloat16), grad_up)


def solution(mesh):
    finer = Mesh(mesh.devices.reshape(12, 8, 4, 2), ("fs_0", "fs_1", "tp_0", "tp_1"))
    return jax.shard_map(
        local,
        mesh=finer,
        in_specs=(P(FS, TP), P(FS, TP), P(FS, None), P(FS, TP), P(FS, TP)),
        out_specs=(P(FS, TP), P(FS, TP)),
        check_vma=False,
    )
```

profile of v0, /device:TPU:8, one launch (start us, length us, event | category | flops | bytes accessed | tf_op | source)
XLA Modules:
  0.0 276.8 jit_solution(1351811485569322641)
XLA Ops:
  7.2 0.0 copy-start
  7.2 0.0 all-gather.7.cloned.1.call-start
  7.2 0.7 broadcast_in_dim.14
  8.0 9.6 %all_to_all.5 = bf16[8,22,128]{2,1,0:T(8,128)(2,1)S(1)} all-to-all(bf16[8,22,128]{2,1,0:T(8,128)(2,1)S(1)} %broadcast_in_dim.14), channel_id=1, replica_groups=mesh['fs_0'=12,'fs_1'=8,'tp_0'=4,'tp_1'=2] {'tp_0','tp_1'}, dimensions={0} | all-to-all | bytes 90112 | tf_op jit(solution)/shard_map/all_to_all | solution.py:46
  17.6 0.7 reshape.33
  18.3 0.0 all-gather.7.cloned.1.call-update
  18.3 0.0 reduce-scatter.5.cloned.1.call-start
  18.3 0.9 fusion.2
  19.3 12.7 %all-gather = bf16[1280,128]{1,0:T(8,128)(2,1)S(1)} all-gather(bf16[320,128]{1,0:T(8,128)(2,1)S(1)} %get-tuple-element.2), channel_id=2, replica_groups=mesh['fs_0'=12,'fs_1'=8,'tp_0'=4,'tp_1'=2] {'tp_0'}, dimensions={0}, use_global_device_ids=true | all-gather | bytes 409600 | tf_op jit(solution)/shard_map/all_gather | solution.py:19
  32.0 2.3 all_gather.22
  34.3 1.9 all-gather.1
  36.2 13.9 %all_gather.24 = bf16[8,320,128]{2,1,0:T(8,128)(2,1)S(1)} all-gather(bf16[2,320,128]{2,1,0:T(8,128)(2,1)S(1)} %bitcast.34), channel_id=1, replica_groups=mesh['fs_0'=12,'fs_1'=8,'tp_0'=4,'tp_1'=2] {'tp_0'}, dimensions={0}, use_global_device_ids=true | all-gather | bytes 819200 | tf_op jit(solution)/shard_map/all_gather | solution.py:19
  50.1 0.1 maximum_bitcast_fusion
  50.2 0.7 copy.18
  50.9 98.5 %all-gather.7.cloned.1.call-done = bf16[96,22,1024]{2,1,0:T(8,128)(2,1)} async-done(((bf16[1,22,1024]{2,1,0:T(8,128)(2,1)}), bf16[96,22,1024]{2,1,0:T(8,128)(2,1)}) %all-gather.7.cloned.1.call-update) | async-done | bytes 4325392 | tf_op jit(solution)/shard_map/all_gather | solution.py:89
  149.4 7.2 %reshape.34 = bf16[2112,1024]{1,0:T(8,128)(2,1)} reshape(bf16[96,22,1024]{2,1,0:T(8,128)(2,1)} %all-gather.7.cloned.1.call-done) | data formatting | bytes 8650752
  156.5 6.7 %fusion.1 = bf16[640,2112]{0,1:T(8,128)(2,1)S(1)} fusion(bf16[640,2112]{0,1:T(8,128)(2,1)} %param.7, bf16[2112,1024]{1,0:T(8,128)(2,1)} %reshape.34, bf16[640,1024]{0,1:T(8,128)(2,1)S(1)} %bitcast.32), kind=kOutput, calls=%fused_computation.2 | convolution fusion | flops 2774999040 | bytes 11042816 | tf_op jit(solution)/shard_map/dot_general | solution.py:79
  163.2 1.5 copy-done.1
  164.7 0.9 fusion.3
  165.6 0.0 copy-start.3
  165.6 0.1 reshape_reshape.7
  165.7 1.1 copy.21
  166.8 0.0 reduce-scatter.5.cloned.1.call-update
  166.8 0.0 reduce-scatter.7.cloned.1.call-start
  166.9 21.0 %all-gather.4 = bf16[12,22,128]{2,1,0:T(8,128)(2,1)S(1)} all-gather(bf16[1,22,128]{2,1,0:T(8,128)(2,1)S(1)} %bitcast.36), channel_id=4, replica_groups=mesh['fs_0'=12,'fs_1'=8,'tp_0'=4,'tp_1'=2] {'fs_0'}, dimensions={0}, use_global_device_ids=true | all-gather | bytes 73216 | tf_op jit(solution)/shard_map/all_gather | solution.py:19
  187.9 27.1 %all_gather.27 = bf16[96,22,128]{2,1,0:T(8,128)(2,1)S(1)} all-gather(bf16[12,22,128]{2,1,0:T(8,128)(2,1)S(1)} %all-gather.4), channel_id=1, replica_groups=mesh['fs_0'=12,'fs_1'=8,'tp_0'=4,'tp_1'=2] {'fs_1'}, dimensions={0}, use_global_device_ids=true | all-gather | bytes 608256 | tf_op jit(solution)/shard_map/all_gather | solution.py:19
  215.0 0.1 copy.23
  215.1 1.0 reshape_reshape.6
  216.0 0.0 reduce-scatter.7.cloned.1.call-update
  216.1 2.6 convolution_convert_fusion
  218.7 50.2 %reduce-scatter.7.cloned.1.call-done = f32[1,22,128]{2,1,0:T(8,128)} async-done(((f32[12,22,128]{2,1,0:T(8,128)}), f32[1,22,128]{2,1,0:T(8,128)}) %reduce-scatter.7.cloned.1.call-update) | async-done | bytes 11280
  268.9 1.3 multiply_bitcast_fusion
  (8 shorter events, 0.1 us)
Async XLA Ops:
  7.2 157.6 %copy-start = (bf16[640,128]{1,0:T(8,128)(2,1)S(1)}, bf16[640,128]{1,0:T(8,128)(2,1)}, u32[]{:S(2)}) copy-start(bf16[640,128]{1,0:T(8,128)(2,1)} %param.6) | copy-start | bytes 491524
  7.2 142.2 %all-gather.7.cloned.1.call-start = ((), (), s32[]{:S(2)}) async-start(), calls=%async_computation.4 | async-start | bytes 4767744 | tf_op jit(solution)/shard_map/all_gather | solution.py:89
  18.3 197.8 %reduce-scatter.5.cloned.1.call-start = ((), (), s32[]{:S(2)}) async-start(), calls=%async_computation.3 | async-start | bytes 1327104 | tf_op jit(solution)/shard_map/reduce_scatter | solution.py:63
  163.2 1.5 copy-start.1
  165.6 1.3 copy-start.3
  166.8 49.2 %copy-start.2 = (bf16[640,2112]{0,1:T(8,128)(2,1)S(1)}, bf16[640,2112]{0,1:T(8,128)(2,1)}, u32[]{:S(2)}) copy-start(bf16[640,2112]{0,1:T(8,128)(2,1)} %copy-done.1) | copy-start | bytes 8110084
  166.8 102.1 %reduce-scatter.7.cloned.1.call-start = ((), (), s32[]{:S(2)}) async-start(), calls=%async_computation.5 | async-start | bytes 159744
Sparse Core Ops, SparseCore 0:
  18.4 130.9 all-gather.6
  167.0 41.8 reduce-scatter.4
  216.2 52.7 reduce-scatter.6
where the time goes:
time: 277 us
  waiting for transfers between devices  149 us (54%)
  blocking collectives  88.5 us (32%)
  local copies, waits for them, and re-layouts  14.1 us (5%)
  between operations  13.8 us (5%)
  matrix products  10.2 us (4%)
    all_gather x1, waiting for transfers between devices, local(): lax.all_gather(down_whole, FS, axis=0, tiled=True)  98.5 us
    all_gather x6, blocking collectives, gather_in_order(): parts = lax.all_gather(parts, axes[k], axis=0, tiled=True)  78.8 us
    unnamed x4, waiting for transfers between devices  50.3 us
    all_to_all x1, blocking collectives, copy_for_each(): return lax.all_to_all(copies, axis, split_axis=0, concat_axis=0, tiled=True)  9.62 us
    unnamed x10, local copies, waits for them, and re-layouts  9.39 us
    dot_general x1, matrix products, times_rows(): lax.dot_general(left, piece, (((1,), (1,)), ((), ())), preferred_element_...  6.66 us
  transfers between devices with their start and end apart: 3, of which 2 were waited for; matrix products, arithmetic and copies ran while one was open for 2% of the time, Pallas kernels for 0%

commit v1 on v0

v1 whole, which is shorter than its diff:
```python
import functools
import math

import jax
import jax.numpy as jnp
from jax import lax
from jax.experimental import pallas as pl
from jax.experimental.pallas import tpu as pltpu
from jax.sharding import PartitionSpec as P

MESH = pl.DeviceIdType.MESH
F32, BF16 = jnp.float32, jnp.bfloat16
NX, NY, NZ = 4, 8, 12
LAG_X, LAG_U, LAG_C, LAG_R = 2, 2, 5, 9


def body(
    rows, win,
    cot_ref, inp_ref, pre_hbm, wu_ref, wd_ref,
    gi_ref, gu_ref,
    pre, cotf, inpx, wpad, zd, zu, wdx, wux, pret, gpt, sendy, recvy, sendz, recvz, gisend, girecv,
    loc_sem, y_ss, y_rs, c_ss, c_rs, c_fs, i_ss, i_rs, zd_ss, zd_rs, zu_ss, zu_rs,
    x_ss, x_rs, xf_ss, sib_ss, us_ss, us_rs, ry_ss, ry_rs, rz_ss, rz_rs, g_ss, g_rs,
):
    fs, tp = lax.axis_index("fs"), lax.axis_index("tp")
    z, y = lax.div(fs, NY), lax.rem(fs, NY)
    x, c = lax.div(tp, 2), lax.rem(tp, 2)
    xr, xl, xo = lax.rem(x + 1, NX), lax.rem(x + NX - 1, NX), lax.rem(x + 2, NX)
    zp, zm = lax.rem(z + 1, NZ), lax.rem(z + NZ - 1, NZ)
    half_z = NZ // 2
    sib = x * 2 + 1 - c
    toks = cot_ref.shape[0]
    tok2 = toks // 2

    def copy(src, dst, ss, rs, to_fs, to_tp):
        return pltpu.make_async_remote_copy(
            src_ref=src, dst_ref=dst, send_sem=ss, recv_sem=rs,
            device_id=(to_fs, to_tp), device_id_type=MESH,
        )

    barrier = pltpu.get_barrier_semaphore()

    def greet(to_fs, to_tp):
        pl.semaphore_signal(barrier, inc=1, device_id=(to_fs, to_tp), device_id_type=MESH)

    def at_y(k):
        return lax.rem(y + k, NY)

    for k in range(1, NY):
        greet(z * NY + at_y(k), tp)
    greet(zp * NY + y, tp)
    greet(zm * NY + y, tp)
    for core in range(2):
        greet(fs, xr * 2 + core)
        greet(fs, xl * 2 + core)
    greet(fs, sib)

    load = pltpu.make_async_copy(pre_hbm, pre, loc_sem)
    load.start()

    keep = lax.broadcasted_iota(jnp.int32, (24, rows), 0) == lax.broadcasted_iota(jnp.int32, (24, rows), 1)
    keep = keep.astype(F32).astype(BF16)
    for k, ref in enumerate((wd_ref, wu_ref)):
        padded = jnp.dot(keep, ref[...], preferred_element_type=F32)
        padded = padded.reshape(3, 8, 128).astype(BF16)
        wpad[k] = padded
    zd[z, pl.ds(y * 3, 3)] = wpad[0]
    zu[z, pl.ds(y * 3, 3)] = wpad[1]

    pl.semaphore_wait(barrier, NY - 1 + 2 + 4 + 1)

    def y_send(k, w):
        buf = (zd, zu)[w]
        return copy(
            wpad.at[w], buf.at[z, pl.ds(y * 3, 3)], y_ss.at[w, k], y_rs.at[w, y], z * NY + at_y(k), tp
        )

    for k in range(1, NY):
        y_send(k, 0).start()

    def lanes(tile):
        return pl.ds(pl.multiple_of(tile * 128, 128), 128)

    def c_part(tile, h):
        return cotf.at[pl.ds(h * tok2, tok2), lanes(tile)]

    def c_own(h, way):
        to = (xr * 2 + c, xl * 2 + c, sib)[way]
        return copy(
            cot_ref.at[pl.ds(h * tok2, tok2)], c_part(tp, h), c_ss.at[h, way], c_rs.at[tp, h], fs, to
        )

    def c_fwd(tile, h, to, slot):
        return copy(c_part(tile, h), c_part(tile, h), c_fs.at[slot], c_rs.at[tile, h], fs, to)

    for h in range(2):
        for way in range(2):
            c_own(h if way == 0 else 1 - h, way).start()
    for k in range(1, NY):
        y_send(k, 1).start()
    for h in range(2):
        c_own(h, 2).start()
    send_inp = copy(inp_ref, inpx, i_ss, i_rs, fs, sib)
    send_inp.start()

    cotf[:, lanes(tp)] = cot_ref[...]

    load.wait()

    def turn(bl, carry):
        first = (c * half_z + bl) * (rows * NY)
        start = pl.multiple_of(jnp.minimum(lax.div(first, 128), (pre.shape[1] - win) // 128) * 128, 128)
        iy = lax.broadcasted_iota(jnp.int32, (NY, 24, win), 0)
        ir = lax.broadcasted_iota(jnp.int32, (NY, 24, win), 1)
        ik = lax.broadcasted_iota(jnp.int32, (NY, 24, win), 2)
        pick = (ik + start == first + iy * rows + ir) & (ir < rows)
        pick = pick.astype(F32).reshape(NY * 24, win).astype(BF16)
        part = pre[:, pl.ds(start, win)]
        turned = lax.dot_general(pick, part, (((1,), (1,)), ((), ())), preferred_element_type=F32)
        pret[bl] = (2.0 * jnp.maximum(turned, 0.0)).astype(BF16)
        return carry

    lax.fori_loop(0, half_z, turn, 0)

    def y_recv(k, w):
        ys = at_y(k)
        buf = (zd, zu)[w]
        return copy(
            wpad.at[w], buf.at[z, pl.ds(ys * 3, 3)], y_ss.at[w, k], y_rs.at[w, ys], fs, tp
        )

    def block_of(t, sign):
        s = lax.div(t + 1, 2)
        odd = lax.rem(t, 2) == 1
        return lax.rem(z + NZ + jnp.where(odd, -s, s) * sign, NZ)

    def ring_copy(buf, b, to_z, ss, rs):
        return copy(buf.at[b], buf.at[b], ss, rs.at[b], to_z * NY + y, tp)

    def ring_step(buf, t, sign, ss, rs):
        b = block_of(t, sign)
        up, down = (zp, zm) if sign > 0 else (zm, zp)

        @pl.when(t > 0)
        def _():
            ring_copy(buf, b, zp, ss.at[b], rs).wait_recv()

        @pl.when(t == 0)
        def _():
            ring_copy(buf, b, up, ss.at[NZ], rs).start()

        @pl.when(t < NZ - 2)
        def _():
            to = jnp.where(lax.rem(t, 2) == 1, up, down)
            ring_copy(buf, b, to, ss.at[b], rs).start()

        return b

    def wd_part(tile, bl):
        return wdx.at[tile, bl]

    def x_send(b, way):
        h, bl = lax.div(b, half_z), lax.rem(b, half_z)
        to = (xr, xl)[way] * 2 + h
        return copy(zd.at[b], wd_part(tp, bl), x_ss.at[way, b], x_rs.at[tp, bl], fs, to)

    def sib_send(b):
        bl = lax.rem(b, half_z)
        return copy(zd.at[b], wd_part(tp, bl), sib_ss.at[b], x_rs.at[tp, bl], fs, sib)

    def us_send(b):
        bl = lax.rem(b, half_z)
        return copy(zu.at[b], wux.at[c, bl], us_ss.at[b], us_rs.at[bl], fs, sib)

    def in_half(b):
        return lax.div(b, half_z) == c

    def down_step(t):
        b = ring_step(zd, t, 1, zd_ss, zd_rs)
        for way in range(2):
            x_send(b, way).start()

        @pl.when(jnp.logical_not(in_half(b)))
        def _():
            sib_send(b).start()

        @pl.when(in_half(b))
        def _():
            wdx[tp, lax.rem(b, half_z)] = zd[b]

    def up_step(t):
        b = ring_step(zu, t, -1, zu_ss, zu_rs)

        @pl.when(jnp.logical_not(in_half(b)))
        def _():
            us_send(b).start()

        @pl.when(in_half(b))
        def _():
            wux[c, lax.rem(b, half_z)] = zu[b]

    def x_sides(bl, core):
        even = lax.rem(bl + core, 2) == 0
        return jnp.where(even, xl, xr), jnp.where(even, xr, xl)

    def x_forward(bl, core):
        src, dst = x_sides(bl, core)
        tile = src * 2 + core
        return copy(
            wd_part(tile, bl), wd_part(tile, bl), xf_ss.at[core, bl], x_rs.at[tile, bl], fs, dst * 2 + c
        )

    def x_wait(tile, bl):
        copy(wd_part(tile, bl), wd_part(tile, bl), xf_ss.at[0, 0], x_rs.at[tile, bl], fs, tp).wait_recv()

    def x_step(t):
        b = block_of(t, 1)

        @pl.when(in_half(b))
        def _():
            bl = lax.rem(b, half_z)
            for core in range(2):
                fwd = x_forward(bl, core)
                fwd.wait_recv()
                fwd.start()

    def piece(bl, ky, core):
        yt = at_y(ky)
        b = c * half_z + bl
        return copy(
            sendy.at[bl, core, yt], recvy.at[y, b], ry_ss.at[bl, core, ky], ry_rs.at[y, b],
            z * NY + yt, x * 2 + core,
        )

    def compute_step(t):
        b = block_of(t, 1)

        @pl.when(in_half(b))
        def _():
            bl = lax.rem(b, half_z)
            for core in range(2):
                x_wait(x_sides(bl, core)[1] * 2 + core, bl)
                x_wait(xo * 2 + core, bl)
            x_wait(sib, bl)
            w = jnp.concatenate([wdx[k, bl].reshape(NY * 24, 128) for k in range(2 * NX)], axis=1)
            gh = lax.dot_general(w, cotf[...], (((1,), (1,)), ((), ())), preferred_element_type=F32)
            gp = (gh * pret[bl].astype(F32)).astype(BF16)
            gpt[bl] = gp
            for core in range(2):
                @pl.when(c == core)
                def _():
                    own = jnp.dot(gp, inp_ref[...], preferred_element_type=F32)
                    other = jnp.dot(gp, inpx[...], preferred_element_type=F32)
                    sendy[bl, core] = own.reshape(NY, 3, 8, 128).astype(BF16)
                    sendy[bl, 1 - core] = other.reshape(NY, 3, 8, 128).astype(BF16)
            recvy[y, b] = sendy[bl, c, y]
            for ky in range(1, NY):
                for core in range(2):
                    piece(bl, ky, core).start()
            piece(bl, 0, 1 - c).start()

    def z_piece(b):
        return copy(sendz.at[b], recvz.at[z], rz_ss.at[b], rz_rs.at[z], b * NY + y, tp)

    def reduce_step(t):
        b = block_of(t, 1)
        own = in_half(b)
        for ky in range(NY):
            ys = at_y(ky)
            wait = copy(sendy.at[0, 0, 0], recvy.at[ys, b], ry_ss.at[0, 0, 0], ry_rs.at[ys, b], fs, tp)
            if ky == 0:
                @pl.when(jnp.logical_not(own))
                def _():
                    wait.wait_recv()
            else:
                wait.wait_recv()
        total = recvy[0, b].astype(F32)
        for k in range(1, NY):
            total = total + recvy[k, b].astype(F32)
        sendz[b] = total.astype(BF16)

        @pl.when(t == 0)
        def _():
            recvz[z] = sendz[b]

        @pl.when(t > 0)
        def _():
            z_piece(b).start()

    for k in range(1, NY):
        y_recv(k, 0).wait_recv()
    down_step(0)

    def c_wait(tile, h):
        c_fwd(tile, h, sib, 0).wait_recv()

    def c_step_one():
        for h in range(2):
            left, right = xl * 2 + c, xr * 2 + c
            c_wait(left, h)
            if h == 0:
                c_fwd(left, h, xr * 2 + c, 0).start()
            c_fwd(left, h, sib, 1 + h).start()
            c_wait(right, 1 - h)
            if h == 0:
                c_fwd(right, 1, xl * 2 + c, 3).start()
            c_fwd(right, 1 - h, sib, 4 + h).start()

    def c_step_two():
        far = xo * 2 + c
        for h in range(2):
            c_wait(far, h)
            c_fwd(far, h, sib, 6 + h).start()

    def c_step_three():
        for k in range(NX):
            for h in range(2):
                c_wait(lax.rem(x + k, NX) * 2 + 1 - c, h)
        send_inp.wait_recv()

    def run(t, carry):
        @pl.when((t > 0) & (t < NZ))
        def _():
            down_step(t)

        @pl.when(t == 1)
        def _():
            c_step_one()
            for k in range(1, NY):
                y_recv(k, 1).wait_recv()

        @pl.when(t == 3)
        def _():
            c_step_two()

        @pl.when(t == LAG_C)
        def _():
            c_step_three()

        @pl.when((t >= LAG_X) & (t < NZ + LAG_X))
        def _():
            x_step(t - LAG_X)

        @pl.when((t >= LAG_U) & (t < NZ + LAG_U))
        def _():
            up_step(t - LAG_U)

        @pl.when((t >= LAG_C) & (t < NZ + LAG_C))
        def _():
            compute_step(t - LAG_C)

        @pl.when(t >= LAG_R)
        def _():
            reduce_step(t - LAG_R)

        return carry

    lax.fori_loop(0, NZ + LAG_C, run, 0)

    def up_wait(bl, carry):
        copy(wux.at[0, bl], wux.at[0, bl], us_ss.at[0], us_rs.at[bl], fs, tp).wait_recv()
        return carry

    lax.fori_loop(0, half_z, up_wait, 0)

    def gi_part(core):
        total = None
        for bl in range(half_z):
            gp = jnp.transpose(gpt[bl].astype(F32)).astype(BF16)
            term = jnp.dot(gp, wux[core, bl].reshape(NY * 24, 128), preferred_element_type=F32)
            total = term if total is None else total + term
        return total

    gisend[...] = gi_part(1 - c)
    own_part = gi_part(c)
    send_gi = copy(gisend, girecv, g_ss, g_rs, fs, sib)
    send_gi.start()

    def rest(t, carry):
        reduce_step(t)
        return carry

    lax.fori_loop(NZ + LAG_C - LAG_R, NZ, rest, 0)

    send_gi.wait_recv()
    gi_ref[...] = (own_part + girecv[...]).astype(BF16)

    def z_wait(t, carry):
        b = block_of(t, 1)
        copy(sendz.at[0], recvz.at[b], rz_ss.at[0], rz_rs.at[b], fs, tp).wait_recv()
        return carry

    lax.fori_loop(1, NZ, z_wait, 0)
    total = recvz[0].astype(F32)
    for k in range(1, NZ):
        total = total + recvz[k].astype(F32)
    scale = 1.0 / math.sqrt(toks * NY * NZ)
    gu_ref[...] = total.reshape(24, 128)[:rows] * scale

    for k in range(1, NY):
        for w in range(2):
            y_send(k, w).wait_send()
    for h in range(2):
        for way in range(3):
            c_own(h, way).wait_send()
    for slot in range(8):
        c_fwd(tp, 0, sib, slot).wait_send()
    send_inp.wait_send()
    send_gi.wait_send()

    def drain(t, carry):
        b = block_of(t, 1)
        for buf, ss, rs in ((zd, zd_ss, zd_rs), (zu, zu_ss, zu_rs)):
            @pl.when(t == 0)
            def _():
                ring_copy(buf, b, zp, ss.at[NZ], rs).wait_send()
        bu = block_of(t, -1)

        @pl.when(t < NZ - 2)
        def _():
            ring_copy(zd, b, zp, zd_ss.at[b], zd_rs).wait_send()
            ring_copy(zu, bu, zp, zu_ss.at[bu], zu_rs).wait_send()

        for way in range(2):
            x_send(b, way).wait_send()

        @pl.when(jnp.logical_not(in_half(b)))
        def _():
            sib_send(b).wait_send()
            us_send(b).wait_send()

        @pl.when(t > 0)
        def _():
            z_piece(b).wait_send()

        return carry

    lax.fori_loop(0, NZ, drain, 0)

    def drain_pieces(bl, carry):
        for core in range(2):
            x_forward(bl, core).wait_send()
        for ky in range(1, NY):
            for core in range(2):
                piece(bl, ky, core).wait_send()
        piece(bl, 0, 1 - c).wait_send()
        return carry

    lax.fori_loop(0, half_z, drain_pieces, 0)


def local(cotangent, inputs, pre_act, w_up, w_down):
    toks, cols = cotangent.shape
    rows = w_down.shape[0]
    ff = pre_act.shape[1]
    half = NZ // 2
    hid = 24 * NY
    win = ff - (ff - (rows * NY + 127)) // 128 * 128
    vmem, dma = pltpu.VMEM, pltpu.SemaphoreType.DMA
    blk = (3 * NY, 8, 128)
    kernel = functools.partial(body, rows, win)
    return tuple(
        pl.pallas_call(
            kernel,
            out_shape=(
                jax.ShapeDtypeStruct((toks, cols), BF16),
                jax.ShapeDtypeStruct((rows, cols), F32),
            ),
            in_specs=[
                pl.BlockSpec(memory_space=vmem),
                pl.BlockSpec(memory_space=vmem),
                pl.BlockSpec(memory_space=pl.ANY),
                pl.BlockSpec(memory_space=vmem),
                pl.BlockSpec(memory_space=vmem),
            ],
            out_specs=(pl.BlockSpec(memory_space=vmem), pl.BlockSpec(memory_space=vmem)),
            scratch_shapes=[
                vmem((toks, ff), BF16),
                vmem((toks, 128 * 2 * NX), BF16),
                vmem((toks, 128), BF16),
                vmem((2, 3, 8, 128), BF16),
                vmem((NZ, *blk), BF16),
                vmem((NZ, *blk), BF16),
                vmem((2 * NX, half, *blk), BF16),
                vmem((2, half, *blk), BF16),
                vmem((half, hid, toks), BF16),
                vmem((half, hid, toks), BF16),
                vmem((half, 2, NY, 3, 8, 128), BF16),
                vmem((NY, NZ, 3, 8, 128), BF16),
                vmem((NZ, 3, 8, 128), BF16),
                vmem((NZ, 3, 8, 128), BF16),
                vmem((toks, 128), F32),
                vmem((toks, 128), F32),
                dma,
                dma((2, NY)), dma((2, NY)),
                dma((2, 3)), dma((2 * NX, 2)), dma((8,)),
                dma, dma,
                dma((NZ + 1,)), dma((NZ,)), dma((NZ + 1,)), dma((NZ,)),
                dma((2, NZ)), dma((2 * NX, half)), dma((2, half)), dma((NZ,)), dma((NZ,)), dma((half,)),
                dma((half, 2, NY)), dma((NY, NZ)), dma((NZ,)), dma((NZ,)), dma, dma,
            ],
            compiler_params=pltpu.CompilerParams(collective_id=0, has_side_effects=True),
        )(cotangent, inputs, pre_act, w_up, w_down)
    )


def solution(mesh):
    return jax.shard_map(
        local,
        mesh=mesh,
        in_specs=(P("fs", "tp"), P("fs", "tp"), P("fs", None), P("fs", "tp"), P("fs", "tp")),
        out_specs=(P("fs", "tp"), P("fs", "tp")),
        check_vma=False,
    )
```

time: 277 us -> 78.4 us (0.28)
  the two profiles are of different devices: /device:TPU:8 before, /device:TPU:1 now
where the time goes in v1:
time: 78.4 us; the launch traced here: 78.1 us
  Pallas kernels  69.2 us (88%)
  local copies, waits for them, and re-layouts  8.23 us (10%)
    pallas_call x1, Pallas kernels, local(): pl.pallas_call(kernel, out_shape=(jax.ShapeDtypeStruct((toks, cols), BF16...  69.2 us
    unnamed x3, local copies, waits for them, and re-layouts  8.23 us

profile of v1, /device:TPU:1, one launch (start us, length us, event | category | flops | bytes accessed | tf_op | source)
XLA Modules:
  0.0 78.1 jit_solution(12031935702194576452)
XLA Ops:
  0.6 5.3 %copy.7.pre_hbm = bf16[640,2112]{1,0:T(8,128)(2,1)} copy(bf16[640,2112]{0,1:T(8,128)(2,1)} %param.7) | data formatting | bytes 5406720 | tf_op args[2]
  6.0 69.2 %shard_map.68 = (bf16[640,128]{1,0:T(8,128)(2,1)}, f32[22,128]{1,0:T(8,128)}) custom-call(bf16[640,128]{1,0:T(8,128)(2,1)} %cot_ref.1, bf16[640,128]{1,0:T(8,128)(2,1)} %inp_ref.1, bf16[640,2112]{1,0:T(8,128)(2,1)} %copy.7.pre_hbm, bf16[22,128]{1,0:T(8,128)(2,1)} %wu_ref.1, bf16[22,128]{1,0:T(8,128)(2,1)} %wd_ref.1), custom_call_target="tpu_custom_call" | custom-call | tf_op jit(solution)/shard_map/pallas_call | solution.py:463
  75.2 1.6 %copy.10 = bf16[640,128]{1,0:T(8,128)(2,1)} copy(bf16[640,128]{1,0:T(8,128)(2,1)} %get-tuple-element.4) | data formatting | bytes 327680
  76.8 1.3 %copy.11 = f32[22,128]{1,0:T(8,128)} copy(f32[22,128]{1,0:T(8,128)} %get-tuple-element.5) | data formatting | bytes 22528

commit v2 on v1

v2 whole, which is shorter than its diff:
```python
import functools
import math

import jax
import jax.numpy as jnp
from jax import lax
from jax.experimental import pallas as pl
from jax.experimental.pallas import tpu as pltpu
from jax.sharding import PartitionSpec as P

MESH = pl.DeviceIdType.MESH
F32, BF16 = jnp.float32, jnp.bfloat16
NX, NY, NZ = 4, 8, 12
LAG_X, LAG_U, LAG_C, LAG_R = 2, 1, 5, 12


def body(
    rows,
    cot_hbm, inp_hbm, pre_hbm, wu_hbm, wd_hbm,
    gi_ref, gu_ref,
    cot_ref, inp_ref, wu_ref, wd_ref, pre, cotf, inpx, wpad, zd, zu, wdx, wux, pret, gpt, sendy, recvy, sendz, recvz, gisend, girecv,
    load_sem, y_ss, y_rs, c_ss, c_rs, i_ss, i_rs, ring_ss, zd_rs, zu_rs,
    x_ss, x_rs, us_rs, ry_ss, ry_rs, rz_ss, rz_rs, g_ss, g_rs,
):
    fs, tp = lax.axis_index("fs"), lax.axis_index("tp")
    z, y = lax.div(fs, NY), lax.rem(fs, NY)
    x, c = lax.div(tp, 2), lax.rem(tp, 2)
    xr, xl, xo = lax.rem(x + 1, NX), lax.rem(x + NX - 1, NX), lax.rem(x + 2, NX)
    zp, zm = lax.rem(z + 1, NZ), lax.rem(z + NZ - 1, NZ)
    half_z = NZ // 2
    sib = x * 2 + 1 - c
    toks = cot_ref.shape[0]
    tok2 = toks // 2
    hid = rows * NY

    def copy(src, dst, ss, rs, to_fs, to_tp):
        return pltpu.make_async_remote_copy(
            src_ref=src, dst_ref=dst, send_sem=ss, recv_sem=rs,
            device_id=(to_fs, to_tp), device_id_type=MESH,
        )

    barrier = pltpu.get_barrier_semaphore()

    def greet(to_fs, to_tp):
        pl.semaphore_signal(barrier, inc=1, device_id=(to_fs, to_tp), device_id_type=MESH)

    def at_y(k):
        return lax.rem(y + k, NY)

    for k in range(1, NY):
        greet(z * NY + at_y(k), tp)
    greet(zp * NY + y, tp)
    greet(zm * NY + y, tp)
    for core in range(2):
        greet(fs, xr * 2 + core)
        greet(fs, xl * 2 + core)
    greet(fs, sib)

    own_pre = pre_hbm.at[pl.ds(c * (half_z * hid), half_z * hid)]
    loads = [
        pltpu.make_async_copy(src, dst, load_sem.at[k])
        for k, (src, dst) in enumerate(
            ((wd_hbm, wd_ref), (wu_hbm, wu_ref), (cot_hbm, cot_ref), (inp_hbm, inp_ref), (own_pre, pre))
        )
    ]
    for load in loads:
        load.start()

    keep = lax.broadcasted_iota(jnp.int32, (24, rows), 0) == lax.broadcasted_iota(jnp.int32, (24, rows), 1)
    keep = keep.astype(F32).astype(BF16)
    for k, ref in enumerate((wd_ref, wu_ref)):
        loads[k].wait()
        padded = jnp.dot(keep, ref[...], preferred_element_type=F32)
        padded = padded.reshape(3, 8, 128).astype(BF16)
        wpad[k] = padded
    zd[z, pl.ds(y * 3, 3)] = wpad[0]
    zu[z, pl.ds(y * 3, 3)] = wpad[1]

    pl.semaphore_wait(barrier, NY - 1 + 2 + 4 + 1)

    def y_send(k, w):
        buf = (zd, zu)[w]
        return copy(
            wpad.at[w], buf.at[z, pl.ds(y * 3, 3)], y_ss, y_rs.at[w], z * NY + at_y(k), tp
        )

    for k in range(1, NY):
        y_send(k, 0).start()

    def lanes(tile):
        return pl.ds(pl.multiple_of(tile * 128, 128), 128)

    def c_part(tile, h):
        return cotf.at[pl.ds(h * tok2, tok2), lanes(tile)]

    def c_own(h, way):
        to = (xr * 2 + c, xl * 2 + c, sib)[way]
        return copy(
            cot_ref.at[pl.ds(h * tok2, tok2)], c_part(tp, h), c_ss, c_rs.at[3 if way == 2 else int(way != h)], fs, to
        )

    def c_fwd(tile, h, to, kind):
        return copy(c_part(tile, h), c_part(tile, h), c_ss, c_rs.at[kind], fs, to)

    def c_wait(kind, parts):
        ref = cotf.at[pl.ds(0, tok2), pl.ds(0, 128 * parts)]
        copy(ref, ref, c_ss, c_rs.at[kind], fs, tp).wait_recv()

    loads[2].wait()
    for h in range(2):
        for way in range(2):
            c_own(h if way == 0 else 1 - h, way).start()
    for k in range(1, NY):
        y_send(k, 1).start()
    for h in range(2):
        c_own(h, 2).start()
    loads[3].wait()
    send_inp = copy(inp_ref, inpx, i_ss, i_rs, fs, sib)
    send_inp.start()

    cotf[:, lanes(tp)] = cot_ref[...]

    loads[4].wait()
    iy = lax.broadcasted_iota(jnp.int32, (NY, 24, hid), 0)
    ir = lax.broadcasted_iota(jnp.int32, (NY, 24, hid), 1)
    ik = lax.broadcasted_iota(jnp.int32, (NY, 24, hid), 2)
    pick = ((ik == iy * rows + ir) & (ir < rows)).astype(F32).reshape(NY * 24, hid).astype(BF16)

    def spread(bl, carry):
        part = pre[pl.ds(pl.multiple_of(bl * hid, 16), hid)]
        part = jnp.dot(pick, part, preferred_element_type=F32)
        pret[bl] = (2.0 * jnp.maximum(part, 0.0)).astype(BF16)
        return carry

    lax.fori_loop(0, half_z, spread, 0)

    def y_wait(w):
        buf = (zd, zu)[w]
        parts = buf.at[0, pl.ds(0, 3 * (NY - 1))]
        copy(parts, parts, y_ss, y_rs.at[w], fs, tp).wait_recv()

    def block_of(t, sign):
        s = lax.div(t + 1, 2)
        odd = lax.rem(t, 2) == 1
        return lax.rem(z + NZ + jnp.where(odd, -s, s) * sign, NZ)

    def ring_copy(buf, b, to_z, rs):
        return copy(buf.at[b], buf.at[b], ring_ss, rs.at[b], to_z * NY + y, tp)

    def ring_step(buf, t, sign, rs):
        b = block_of(t, sign)
        up, down = (zp, zm) if sign > 0 else (zm, zp)

        @pl.when(t > 0)
        def _():
            ring_copy(buf, b, zp, rs).wait_recv()

        @pl.when(t == 0)
        def _():
            ring_copy(buf, b, up, rs).start()

        @pl.when(t < NZ - 2)
        def _():
            to = jnp.where(lax.rem(t, 2) == 1, up, down)
            ring_copy(buf, b, to, rs).start()

        return b

    def wd_part(tile, bl):
        return wdx.at[tile * half_z + bl]

    def via_right(bl, core):
        return lax.rem(bl + core, 2) == 0

    def x_send(b, way):
        h, bl = lax.div(b, half_z), lax.rem(b, half_z)
        to = (xr, xl)[way] * 2 + h
        kind = jnp.where(via_right(bl, c) == (way == 0), 0, 1)
        return copy(zd.at[b], wd_part(tp, bl), x_ss, x_rs.at[kind, bl], fs, to)

    def sib_send(b):
        bl = lax.rem(b, half_z)
        return copy(zd.at[b], wd_part(tp, bl), x_ss, x_rs.at[1, bl], fs, sib)

    def us_send(b):
        bl = lax.rem(b, half_z)
        return copy(zu.at[b], wux.at[c, bl], x_ss, us_rs, fs, sib)

    def in_half(b):
        return lax.div(b, half_z) == c

    def down_step(t):
        b = ring_step(zd, t, 1, zd_rs)
        for way in range(2):
            x_send(b, way).start()

        @pl.when(jnp.logical_not(in_half(b)))
        def _():
            sib_send(b).start()

        @pl.when(in_half(b))
        def _():
            wdx[tp * half_z + lax.rem(b, half_z)] = zd[b]

    def up_step(t):
        b = ring_step(zu, t, -1, zu_rs)

        @pl.when(jnp.logical_not(in_half(b)))
        def _():
            us_send(b).start()

        @pl.when(in_half(b))
        def _():
            wux[c, lax.rem(b, half_z)] = zu[b]

    def x_forward(bl, core):
        right = via_right(bl, core)
        src, dst = jnp.where(right, xl, xr), jnp.where(right, xr, xl)
        part = wd_part(src * 2 + core, bl)
        return copy(part, part, x_ss, x_rs.at[1, bl], fs, dst * 2 + c)

    def x_wait(kind, bl, parts):
        ref = wdx.at[pl.ds(0, parts)]
        copy(ref, ref, x_ss, x_rs.at[kind, bl], fs, tp).wait_recv()

    def x_step(t):
        b = block_of(t, 1)

        @pl.when(in_half(b))
        def _():
            bl = lax.rem(b, half_z)
            x_wait(0, bl, 2)
            for core in range(2):
                x_forward(bl, core).start()

    def piece(bl, ky, core):
        yt = at_y(ky)
        b = c * half_z + bl
        return copy(
            sendy.at[bl, core, yt], recvy.at[b, y], ry_ss, ry_rs.at[b],
            z * NY + yt, x * 2 + core,
        )

    def compute_step(t):
        b = block_of(t, 1)

        @pl.when(in_half(b))
        def _():
            bl = lax.rem(b, half_z)
            x_wait(1, bl, 5)
            w = jnp.concatenate([wdx[k * half_z + bl].reshape(NY * 24, 128) for k in range(2 * NX)], axis=1)
            gh = lax.dot_general(w, cotf[...], (((1,), (1,)), ((), ())), preferred_element_type=F32)
            gp = (gh * pret[bl].astype(F32)).astype(BF16)
            gpt[bl] = gp
            for core in range(2):
                @pl.when(c == core)
                def _():
                    own = jnp.dot(gp, inp_ref[...], preferred_element_type=F32)
                    other = jnp.dot(gp, inpx[...], preferred_element_type=F32)
                    sendy[bl, core] = own.reshape(NY, 3, 8, 128).astype(BF16)
                    sendy[bl, 1 - core] = other.reshape(NY, 3, 8, 128).astype(BF16)
            recvy[b, y] = sendy[bl, c, y]
            for ky in range(1, NY):
                for core in range(2):
                    piece(bl, ky, core).start()
            piece(bl, 0, 1 - c).start()

    def z_piece(b):
        return copy(sendz.at[b], recvz.at[z], rz_ss, rz_rs, b * NY + y, tp)

    def reduce_step(t):
        b = block_of(t, 1)
        own = in_half(b)
        for count, when in ((NY - 1, own), (NY, jnp.logical_not(own))):
            @pl.when(when)
            def _():
                ref = recvy.at[b, pl.ds(0, count)]
                copy(ref, ref, ry_ss, ry_rs.at[b], fs, tp).wait_recv()

        total = recvy[b, 0].astype(F32)
        for k in range(1, NY):
            total = total + recvy[b, k].astype(F32)
        sendz[b] = total.astype(BF16)

        @pl.when(t == 0)
        def _():
            recvz[z] = sendz[b]

        @pl.when(t > 0)
        def _():
            z_piece(b).start()

    left, right = xl * 2 + c, xr * 2 + c

    def c_step_one():
        c_wait(0, 2)
        c_fwd(left, 0, xr * 2 + c, 2).start()
        c_fwd(right, 1, xl * 2 + c, 2).start()
        c_fwd(left, 0, sib, 3).start()
        c_fwd(right, 1, sib, 3).start()

    def c_step_half():
        c_wait(1, 2)
        c_fwd(left, 1, sib, 3).start()
        c_fwd(right, 0, sib, 3).start()

    def c_step_two():
        far = xo * 2 + c
        c_wait(2, 2)
        for h in range(2):
            c_fwd(far, h, sib, 3).start()

    def c_step_three():
        c_wait(3, 2 * NX)
        send_inp.wait_recv()

    c_step_one()
    y_wait(0)
    down_step(0)

    def run(t, carry):
        @pl.when((t > 0) & (t < NZ))
        def _():
            down_step(t)

        @pl.when(t == 1)
        def _():
            c_step_half()
            y_wait(1)

        @pl.when(t == 4)
        def _():
            c_step_two()

        @pl.when(t == LAG_C)
        def _():
            c_step_three()

        @pl.when((t >= LAG_X) & (t < NZ + LAG_X))
        def _():
            x_step(t - LAG_X)

        @pl.when((t >= LAG_U) & (t < NZ + LAG_U))
        def _():
            up_step(t - LAG_U)

        @pl.when((t >= LAG_C) & (t < NZ + LAG_C))
        def _():
            compute_step(t - LAG_C)

        @pl.when(t >= LAG_R)
        def _():
            reduce_step(t - LAG_R)

        return carry

    lax.fori_loop(0, NZ + LAG_C, run, 0)

    copy(wux.at[0], wux.at[0], x_ss, us_rs, fs, tp).wait_recv()

    def gi_part(core):
        total = None
        for bl in range(half_z):
            gp = jnp.transpose(gpt[bl].astype(F32)).astype(BF16)
            term = jnp.dot(gp, wux[core, bl].reshape(NY * 24, 128), preferred_element_type=F32)
            total = term if total is None else total + term
        return total

    gisend[...] = gi_part(1 - c)


    def rest(t, carry):
        reduce_step(t)
        return carry

    lax.fori_loop(NZ + LAG_C - LAG_R, NZ, rest, 0)
    send_gi = copy(gisend, girecv, g_ss, g_rs, fs, sib)
    send_gi.start()
    own_part = gi_part(c)

    send_gi.wait_recv()
    gi_ref[...] = (own_part + girecv[...]).astype(BF16)

    others = sendz.at[pl.ds(0, NZ - 1)]
    copy(others, others, rz_ss, rz_rs, fs, tp).wait_recv()
    total = recvz[0].astype(F32)
    for k in range(1, NZ):
        total = total + recvz[k].astype(F32)
    scale = 1.0 / math.sqrt(toks * NY * NZ)
    gu_ref[...] = total.reshape(24, 128)[:rows] * scale

    send_inp.wait_send()
    send_gi.wait_send()
    copy(others, others, rz_ss, rz_rs, fs, tp).wait_send()
    for ref, ss in (
        (zd.at[pl.ds(0, 2), pl.ds(0, 3 * (NY - 1))], y_ss),
        (cotf.at[:, pl.ds(0, 128 * 7)], c_ss),
        (wdx.at[pl.ds(0, 2 * (NZ - 1))], ring_ss),
        (wdx, x_ss),
        (wdx.at[pl.ds(0, 2 * NY - 1), pl.ds(0, 3 * half_z)], ry_ss),
    ):
        copy(ref, ref, ss, g_rs, fs, tp).wait_send()


def local(cotangent, inputs, pre_act, w_up, w_down):
    toks, cols = cotangent.shape
    rows = w_down.shape[0]
    ff = pre_act.shape[1]
    half = NZ // 2
    hid = 24 * NY
    vmem, dma = pltpu.VMEM, pltpu.SemaphoreType.DMA
    blk = (3 * NY, 8, 128)
    kernel = functools.partial(body, rows)
    return tuple(
        pl.pallas_call(
            kernel,
            out_shape=(
                pltpu.VMEM((toks, cols), BF16),
                pltpu.VMEM((rows, cols), F32),
            ),
            in_specs=[
                pl.BlockSpec(memory_space=pl.ANY),
            ] * 5,
            out_specs=(pl.BlockSpec(memory_space=vmem), pl.BlockSpec(memory_space=vmem)),
            scratch_shapes=[
                vmem((toks, cols), BF16),
                vmem((toks, cols), BF16),
                vmem((rows, cols), BF16),
                vmem((rows, cols), BF16),
                vmem((ff // 2, toks), BF16),
                vmem((toks, 128 * 2 * NX), BF16),
                vmem((toks, 128), BF16),
                vmem((2, 3, 8, 128), BF16),
                vmem((NZ, *blk), BF16),
                vmem((NZ, *blk), BF16),
                vmem((2 * NX * half, *blk), BF16),
                vmem((2, half, *blk), BF16),
                vmem((half, hid, toks), BF16),
                vmem((half, hid, toks), BF16),
                vmem((half, 2, NY, 3, 8, 128), BF16),
                vmem((NZ, NY, 3, 8, 128), BF16),
                vmem((NZ, 3, 8, 128), BF16),
                vmem((NZ, 3, 8, 128), BF16),
                vmem((toks, 128), F32),
                vmem((toks, 128), F32),
                dma((5,)),
                dma, dma((2,)), dma, dma((4,)), dma, dma,
                dma, dma((NZ,)), dma((NZ,)),
                dma, dma((2, half)), dma, dma, dma((NZ,)), dma, dma, dma, dma,
            ],
            compiler_params=pltpu.CompilerParams(collective_id=0, has_side_effects=True),
        )(cotangent, inputs, pre_act.T, w_up, w_down)
    )


def solution(mesh):
    return jax.shard_map(
        local,
        mesh=mesh,
        in_specs=(P("fs", "tp"), P("fs", "tp"), P("fs", None), P("fs", "tp"), P("fs", "tp")),
        out_specs=(P("fs", "tp"), P("fs", "tp")),
        check_vma=False,
    )
```

time: 78.4 us -> 67.6 us (0.86)
  local copies, waits for them, and re-layouts: 8.23 us -> 1.27 us
  Pallas kernels: 69.2 us -> 65.5 us
    unnamed x3 -> x2, local copies, waits for them, and re-layouts: 8.23 us -> 1.27 us
    pallas_call x1, Pallas kernels: 69.2 us -> 65.5 us  [local(): pl.pallas_call(kernel, out_shape=(pltpu.VMEM((toks, cols), BF16), pltpu.V...]
where the time goes in v2:
time: 67.6 us; the launch traced here: 67.4 us
  Pallas kernels  65.5 us (97%)
  local copies, waits for them, and re-layouts  1.27 us (2%)
    pallas_call x1, Pallas kernels, local(): pl.pallas_call(kernel, out_shape=(pltpu.VMEM((toks, cols), BF16), pltpu.V...  65.5 us

profile of v2, /device:TPU:1, one launch (start us, length us, event | category | flops | bytes accessed | tf_op | source)
XLA Modules:
  0.0 67.4 jit_solution(4428531545398882910)
XLA Ops:
  0.6 65.5 %shard_map.68 = (bf16[640,128]{1,0:T(8,128)(2,1)S(1)}, f32[22,128]{1,0:T(8,128)S(1)}) custom-call(bf16[640,128]{1,0:T(8,128)(2,1)} %cot_hbm.1, bf16[640,128]{1,0:T(8,128)(2,1)} %inp_hbm.1, bf16[2112,640]{1,0:T(8,128)(2,1)} %bitcast.1, bf16[22,128]{1,0:T(8,128)(2,1)} %wu_hbm.1, bf16[22,128]{1,0:T(8,128)(2,1)} %wd_hbm.1), custom_call_target="tpu_custom_call" | custom-call | tf_op jit(solution)/shard_map/pallas_call | solution.py:415
  66.1 0.7 copy.9
  66.8 0.6 copy.10

commit v3 on v2

--- a/solution.py
+++ b/solution.py
@@ -11,16 +11,16 @@
 MESH = pl.DeviceIdType.MESH
 F32, BF16 = jnp.float32, jnp.bfloat16
 NX, NY, NZ = 4, 8, 12
-LAG_X, LAG_U, LAG_C, LAG_R = 2, 1, 5, 12
+LAG_X, LAG_C, LAG_R = 2, 5, 12
 
 
 def body(
     rows,
     cot_hbm, inp_hbm, pre_hbm, wu_hbm, wd_hbm,
     gi_ref, gu_ref,
-    cot_ref, inp_ref, wu_ref, wd_ref, pre, cotf, inpx, wpad, zd, zu, wdx, wux, pret, gpt, sendy, recvy, sendz, recvz, gisend, girecv,
-    load_sem, y_ss, y_rs, c_ss, c_rs, i_ss, i_rs, ring_ss, zd_rs, zu_rs,
-    x_ss, x_rs, us_rs, ry_ss, ry_rs, rz_ss, rz_rs, g_ss, g_rs,
+    cot_ref, inp_ref, wu_ref, wd_ref, pre, cotf, inpx, wpad, zr, wdx, wux, pret, gpt, sendy, recvy, sendz, recvz, gisend, girecv,
+    load_sem, y_ss, y_rs, c_ss, c_rs, i_ss, i_rs, ring_ss, zr_rs,
+    x_ss, xf_ss, x_rs, us_rs, ry_ss, ry_rs, rz_ss, rz_rs, g_ss, g_rs,
 ):
     fs, tp = lax.axis_index("fs"), lax.axis_index("tp")
     z, y = lax.div(fs, NY), lax.rem(fs, NY)
@@ -48,7 +48,8 @@
         return lax.rem(y + k, NY)
 
     for k in range(1, NY):
-        greet(z * NY + at_y(k), tp)
+        for core in range(2):
+            greet(z * NY + at_y(k), x * 2 + core)
     greet(zp * NY + y, tp)
     greet(zm * NY + y, tp)
     for core in range(2):
@@ -73,19 +74,23 @@
         padded = jnp.dot(keep, ref[...], preferred_element_type=F32)
         padded = padded.reshape(3, 8, 128).astype(BF16)
         wpad[k] = padded
-    zd[z, pl.ds(y * 3, 3)] = wpad[0]
-    zu[z, pl.ds(y * 3, 3)] = wpad[1]
-
-    pl.semaphore_wait(barrier, NY - 1 + 2 + 4 + 1)
+
+    def own_rows(core):
+        return zr.at[core * NZ + z, pl.ds(y * 3, 3)]
+
+    own_rows(c)[...] = wpad[1 - c]
+
+    pl.semaphore_wait(barrier, 2 * (NY - 1) + 2 + 4 + 1)
 
     def y_send(k, w):
-        buf = (zd, zu)[w]
-        return copy(
-            wpad.at[w], buf.at[z, pl.ds(y * 3, 3)], y_ss, y_rs.at[w], z * NY + at_y(k), tp
-        )
+        return copy(wpad.at[w], own_rows(c), y_ss, y_rs, z * NY + at_y(k), x * 2 + 1 - w)
+
+    def y_send_sib():
+        return copy(wpad.at[c], own_rows(c), y_ss, y_rs, fs, sib)
 
     for k in range(1, NY):
         y_send(k, 0).start()
+    y_send_sib().start()
 
     def lanes(tile):
         return pl.ds(pl.multiple_of(tile * 128, 128), 128)
@@ -134,37 +139,33 @@
 
     lax.fori_loop(0, half_z, spread, 0)
 
-    def y_wait(w):
-        buf = (zd, zu)[w]
-        parts = buf.at[0, pl.ds(0, 3 * (NY - 1))]
-        copy(parts, parts, y_ss, y_rs.at[w], fs, tp).wait_recv()
+    def y_parts():
+        ref = zr.at[pl.ds(0, 3), pl.ds(0, 2 * NY - 1)]
+        return copy(ref, ref, y_ss, y_rs, fs, tp)
 
     def block_of(t, sign):
         s = lax.div(t + 1, 2)
         odd = lax.rem(t, 2) == 1
         return lax.rem(z + NZ + jnp.where(odd, -s, s) * sign, NZ)
 
-    def ring_copy(buf, b, to_z, rs):
-        return copy(buf.at[b], buf.at[b], ring_ss, rs.at[b], to_z * NY + y, tp)
-
-    def ring_step(buf, t, sign, rs):
-        b = block_of(t, sign)
-        up, down = (zp, zm) if sign > 0 else (zm, zp)
-
+    ring_sign = jnp.where(c == 1, 1, -1)
+    ring_up, ring_down = jnp.where(c == 1, zp, zm), jnp.where(c == 1, zm, zp)
+
+    def ring_copy(slot, to_z):
+        return copy(zr.at[slot], zr.at[slot], ring_ss, zr_rs.at[slot], to_z * NY + y, tp)
+
+    def ring_step(t, slot):
         @pl.when(t > 0)
         def _():
-            ring_copy(buf, b, zp, rs).wait_recv()
+            ring_copy(slot, zp).wait_recv()
 
         @pl.when(t == 0)
         def _():
-            ring_copy(buf, b, up, rs).start()
+            ring_copy(slot, ring_up).start()
 
         @pl.when(t < NZ - 2)
         def _():
-            to = jnp.where(lax.rem(t, 2) == 1, up, down)
-            ring_copy(buf, b, to, rs).start()
-
-        return b
+            ring_copy(slot, jnp.where(lax.rem(t, 2) == 1, ring_up, ring_down)).start()
 
     def wd_part(tile, bl):
         return wdx.at[tile * half_z + bl]
@@ -172,52 +173,52 @@
     def via_right(bl, core):
         return lax.rem(bl + core, 2) == 0
 
-    def x_send(b, way):
+    def x_send(k, b, way):
         h, bl = lax.div(b, half_z), lax.rem(b, half_z)
         to = (xr, xl)[way] * 2 + h
-        kind = jnp.where(via_right(bl, c) == (way == 0), 0, 1)
-        return copy(zd.at[b], wd_part(tp, bl), x_ss, x_rs.at[kind, bl], fs, to)
-
-    def sib_send(b):
-        bl = lax.rem(b, half_z)
-        return copy(zd.at[b], wd_part(tp, bl), x_ss, x_rs.at[1, bl], fs, sib)
-
-    def us_send(b):
-        bl = lax.rem(b, half_z)
-        return copy(zu.at[b], wux.at[c, bl], x_ss, us_rs, fs, sib)
+        kind = jnp.where(via_right(bl, k) == (way == 0), 0, 1)
+        return copy(zr.at[k * NZ + b], wd_part(x * 2 + k, bl), x_ss, x_rs.at[kind, bl], fs, to)
 
     def in_half(b):
         return lax.div(b, half_z) == c
 
-    def down_step(t):
-        b = ring_step(zd, t, 1, zd_rs)
-        for way in range(2):
-            x_send(b, way).start()
-
-        @pl.when(jnp.logical_not(in_half(b)))
-        def _():
-            sib_send(b).start()
-
-        @pl.when(in_half(b))
-        def _():
-            wdx[tp * half_z + lax.rem(b, half_z)] = zd[b]
-
-    def up_step(t):
-        b = ring_step(zu, t, -1, zu_rs)
-
-        @pl.when(jnp.logical_not(in_half(b)))
-        def _():
-            us_send(b).start()
-
-        @pl.when(in_half(b))
-        def _():
-            wux[c, lax.rem(b, half_z)] = zu[b]
+    def gather_step(t, carry):
+        b = block_of(t, ring_sign)
+        bl = lax.rem(b, half_z)
+        for k in range(2):
+            slot = k * NZ + b
+            ring_step(t, slot)
+
+            @pl.when(c == 1)
+            def _():
+                for way in range(2):
+                    x_send(k, b, way).start()
+
+                @pl.when(in_half(b))
+                def _():
+                    wdx[(x * 2 + k) * half_z + bl] = zr[slot]
+
+                @pl.when(jnp.logical_not(in_half(b)))
+                def _():
+                    copy(zr.at[slot], wd_part(x * 2 + k, bl), xf_ss, x_rs.at[1, bl], fs, sib).start()
+
+            @pl.when(c == 0)
+            def _():
+                @pl.when(in_half(b))
+                def _():
+                    wux[k * half_z + bl] = zr[slot]
+
+                @pl.when(jnp.logical_not(in_half(b)))
+                def _():
+                    copy(zr.at[slot], wux.at[k * half_z + bl], xf_ss, us_rs, fs, sib).start()
+
+        return carry
 
     def x_forward(bl, core):
         right = via_right(bl, core)
         src, dst = jnp.where(right, xl, xr), jnp.where(right, xr, xl)
         part = wd_part(src * 2 + core, bl)
-        return copy(part, part, x_ss, x_rs.at[1, bl], fs, dst * 2 + c)
+        return copy(part, part, xf_ss, x_rs.at[1, bl], fs, dst * 2 + c)
 
     def x_wait(kind, bl, parts):
         ref = wdx.at[pl.ds(0, parts)]
@@ -247,7 +248,11 @@
         @pl.when(in_half(b))
         def _():
             bl = lax.rem(b, half_z)
-            x_wait(1, bl, 5)
+            for core, parts in ((0, 6), (1, 4)):
+                @pl.when(c == core)
+                def _():
+                    x_wait(1, bl, parts)
+
             w = jnp.concatenate([wdx[k * half_z + bl].reshape(NY * 24, 128) for k in range(2 * NX)], axis=1)
             gh = lax.dot_general(w, cotf[...], (((1,), (1,)), ((), ())), preferred_element_type=F32)
             gp = (gh * pret[bl].astype(F32)).astype(BF16)
@@ -315,20 +320,20 @@
         send_inp.wait_recv()
 
     c_step_one()
-    y_wait(0)
-    down_step(0)
+    y_parts().wait_recv()
 
     def run(t, carry):
-        @pl.when((t > 0) & (t < NZ))
-        def _():
-            down_step(t)
+        hop = lax.div(2 * t - 2 + 4, 5)
+        due = (t >= 1) & (lax.div(5 * hop, 2) == t - 1)
+        first = jnp.where(c == 1, jnp.minimum(t, NZ), jnp.maximum(2 * hop - 1, 0))
+        last = jnp.where(c == 1, t + 1, jnp.where(due, 2 * hop + 1, 0))
+        lax.fori_loop(first, jnp.minimum(last, NZ), gather_step, 0)
 
         @pl.when(t == 1)
         def _():
             c_step_half()
-            y_wait(1)
-
-        @pl.when(t == 4)
+
+        @pl.when(t == 3)
         def _():
             c_step_two()
 
@@ -340,15 +345,11 @@
         def _():
             x_step(t - LAG_X)
 
-        @pl.when((t >= LAG_U) & (t < NZ + LAG_U))
-        def _():
-            up_step(t - LAG_U)
-
         @pl.when((t >= LAG_C) & (t < NZ + LAG_C))
         def _():
             compute_step(t - LAG_C)
 
-        @pl.when(t >= LAG_R)
+        @pl.when((t >= LAG_R) & (t < NZ + LAG_R))
         def _():
             reduce_step(t - LAG_R)
 
@@ -356,13 +357,15 @@
 
     lax.fori_loop(0, NZ + LAG_C, run, 0)
 
-    copy(wux.at[0], wux.at[0], x_ss, us_rs, fs, tp).wait_recv()
+    @pl.when(c == 1)
+    def _():
+        copy(wux, wux, x_ss, us_rs, fs, tp).wait_recv()
 
     def gi_part(core):
         total = None
         for bl in range(half_z):
             gp = jnp.transpose(gpt[bl].astype(F32)).astype(BF16)
-            term = jnp.dot(gp, wux[core, bl].reshape(NY * 24, 128), preferred_element_type=F32)
+            term = jnp.dot(gp, wux[core * half_z + bl].reshape(NY * 24, 128), preferred_element_type=F32)
             total = term if total is None else total + term
         return total
 
@@ -393,13 +396,17 @@
     send_gi.wait_send()
     copy(others, others, rz_ss, rz_rs, fs, tp).wait_send()
     for ref, ss in (
-        (zd.at[pl.ds(0, 2), pl.ds(0, 3 * (NY - 1))], y_ss),
+        (zr.at[pl.ds(0, 3), pl.ds(0, 2 * NY - 1)], y_ss),
         (cotf.at[:, pl.ds(0, 128 * 7)], c_ss),
         (wdx.at[pl.ds(0, 2 * (NZ - 1))], ring_ss),
-        (wdx, x_ss),
+        (wdx.at[pl.ds(0, 4 * half_z)], xf_ss),
         (wdx.at[pl.ds(0, 2 * NY - 1), pl.ds(0, 3 * half_z)], ry_ss),
     ):
         copy(ref, ref, ss, g_rs, fs, tp).wait_send()
+
+    @pl.when(c == 1)
+    def _():
+        copy(wdx, wdx, x_ss, g_rs, fs, tp).wait_send()
 
 
 def local(cotangent, inputs, pre_act, w_up, w_down):
@@ -431,10 +438,9 @@
                 vmem((toks, 128 * 2 * NX), BF16),
                 vmem((toks, 128), BF16),
                 vmem((2, 3, 8, 128), BF16),
-                vmem((NZ, *blk), BF16),
-                vmem((NZ, *blk), BF16),
+                vmem((2 * NZ, *blk), BF16),
                 vmem((2 * NX * half, *blk), BF16),
-                vmem((2, half, *blk), BF16),
+                vmem((2 * half, *blk), BF16),
                 vmem((half, hid, toks), BF16),
                 vmem((half, hid, toks), BF16),
                 vmem((half, 2, NY, 3, 8, 128), BF16),
@@ -444,9 +450,9 @@
                 vmem((toks, 128), F32),
                 vmem((toks, 128), F32),
                 dma((5,)),
-                dma, dma((2,)), dma, dma((4,)), dma, dma,
-                dma, dma((NZ,)), dma((NZ,)),
-                dma, dma((2, half)), dma, dma, dma((NZ,)), dma, dma, dma, dma,
+                dma, dma, dma, dma((4,)), dma, dma,
+                dma, dma((2 * NZ,)),
+                dma, dma, dma((2, half)), dma, dma, dma((NZ,)), dma, dma, dma, dma,
             ],
             compiler_params=pltpu.CompilerParams(collective_id=0, has_side_effects=True),
         )(cotangent, inputs, pre_act.T, w_up, w_down)

time: 67.6 us -> 63.3 us (0.936)
  Pallas kernels: 65.5 us -> 61.2 us
    pallas_call x1, Pallas kernels: 65.5 us -> 61.2 us  [local(): pl.pallas_call(kernel, out_shape=(pltpu.VMEM((toks, cols), BF16), pltpu.V...]
where the time goes in v3:
time: 63.3 us; the launch traced here: 63.1 us
  Pallas kernels  61.2 us (97%)
  local copies, waits for them, and re-layouts  1.27 us (2%)
  between operations  0.64 us (1%)
    pallas_call x1, Pallas kernels, local(): pl.pallas_call(kernel, out_shape=(pltpu.VMEM((toks, cols), BF16), pltpu.V...  61.2 us
    unnamed x2, local copies, waits for them, and re-layouts  1.27 us

profile of v3, /device:TPU:1, one launch (start us, length us, event | category | flops | bytes accessed | tf_op | source)
XLA Modules:
  0.0 63.1 jit_solution(3315985931228693357)
XLA Ops:
  0.6 61.2 %shard_map.68 = (bf16[640,128]{1,0:T(8,128)(2,1)S(1)}, f32[22,128]{1,0:T(8,128)S(1)}) custom-call(bf16[640,128]{1,0:T(8,128)(2,1)} %cot_hbm.1, bf16[640,128]{1,0:T(8,128)(2,1)} %inp_hbm.1, bf16[2112,640]{1,0:T(8,128)(2,1)} %bitcast.1, bf16[22,128]{1,0:T(8,128)(2,1)} %wu_hbm.1, bf16[22,128]{1,0:T(8,128)(2,1)} %wd_hbm.1), custom_call_target="tpu_custom_call" | custom-call | tf_op jit(solution)/shard_map/pallas_call | solution.py:422
  61.9 0.7 %copy.9 = bf16[640,128]{1,0:T(8,128)(2,1)} copy(bf16[640,128]{1,0:T(8,128)(2,1)S(1)} %get-tuple-element.2) | data formatting | bytes 327680
  62.5 0.6 copy.10

commit v4 on v3

--- a/solution.py
+++ b/solution.py
@@ -11,7 +11,7 @@
 MESH = pl.DeviceIdType.MESH
 F32, BF16 = jnp.float32, jnp.bfloat16
 NX, NY, NZ = 4, 8, 12
-LAG_X, LAG_C, LAG_R = 2, 5, 12
+LAG_X, LAG_C, LAG_R = 3, 6, 13
 
 
 def body(
@@ -323,8 +323,8 @@
     y_parts().wait_recv()
 
     def run(t, carry):
-        hop = lax.div(2 * t - 2 + 4, 5)
-        due = (t >= 1) & (lax.div(5 * hop, 2) == t - 1)
+        hop = lax.div(1 * (t - 1) + 2, 3)
+        due = (t >= 1) & (lax.div(3 * hop, 1) == t - 1)
         first = jnp.where(c == 1, jnp.minimum(t, NZ), jnp.maximum(2 * hop - 1, 0))
         last = jnp.where(c == 1, t + 1, jnp.where(due, 2 * hop + 1, 0))
         lax.fori_loop(first, jnp.minimum(last, NZ), gather_step, 0)
@@ -355,7 +355,7 @@
 
         return carry
 
-    lax.fori_loop(0, NZ + LAG_C, run, 0)
+    lax.fori_loop(0, 20, run, 0)
 
     @pl.when(c == 1)
     def _():
@@ -376,7 +376,7 @@
         reduce_step(t)
         return carry
 
-    lax.fori_loop(NZ + LAG_C - LAG_R, NZ, rest, 0)
+    lax.fori_loop(20 - LAG_R, NZ, rest, 0)
     send_gi = copy(gisend, girecv, g_ss, g_rs, fs, sib)
     send_gi.start()
     own_part = gi_part(c)

time: 63.3 us -> 62 us (0.979)
  Pallas kernels: 61.2 us -> 60 us
    pallas_call x1, Pallas kernels: 61.2 us -> 60 us  [local(): pl.pallas_call(kernel, out_shape=(pltpu.VMEM((toks, cols), BF16), pltpu.V...]
where the time goes in v4:
time: 62 us; the launch traced here: 61.9 us
  Pallas kernels  60 us (97%)
  local copies, waits for them, and re-layouts  1.27 us (2%)
  between operations  0.64 us (1%)
    pallas_call x1, Pallas kernels, local(): pl.pallas_call(kernel, out_shape=(pltpu.VMEM((toks, cols), BF16), pltpu.V...  60 us
    unnamed x2, local copies, waits for them, and re-layouts  1.27 us

profile of v4, /device:TPU:1, one launch (start us, length us, event | category | flops | bytes accessed | tf_op | source)
XLA Modules:
  0.0 61.9 jit_solution(1136679197664656021)
XLA Ops:
  0.6 60.0 %shard_map.68 = (bf16[640,128]{1,0:T(8,128)(2,1)S(1)}, f32[22,128]{1,0:T(8,128)S(1)}) custom-call(bf16[640,128]{1,0:T(8,128)(2,1)} %cot_hbm.1, bf16[640,128]{1,0:T(8,128)(2,1)} %inp_hbm.1, bf16[2112,640]{1,0:T(8,128)(2,1)} %bitcast.1, bf16[22,128]{1,0:T(8,128)(2,1)} %wu_hbm.1, bf16[22,128]{1,0:T(8,128)(2,1)} %wd_hbm.1), custom_call_target="tpu_custom_call" | custom-call | tf_op jit(solution)/shard_map/pallas_call | solution.py:422
  60.6 0.7 %copy.9 = bf16[640,128]{1,0:T(8,128)(2,1)} copy(bf16[640,128]{1,0:T(8,128)(2,1)S(1)} %get-tuple-element.2) | data formatting | bytes 327680
  61.3 0.6 copy.10

commit v5 on v4

--- a/solution.py
+++ b/solution.py
@@ -11,6 +11,7 @@
 MESH = pl.DeviceIdType.MESH
 F32, BF16 = jnp.float32, jnp.bfloat16
 NX, NY, NZ = 4, 8, 12
+FAR_FIRST = sorted(range(1, NY), key=lambda k: -min(k, NY - k))
 LAG_X, LAG_C, LAG_R = 3, 6, 13
 
 
@@ -47,8 +48,8 @@
     def at_y(k):
         return lax.rem(y + k, NY)
 
-    for k in range(1, NY):
-        for core in range(2):
+    for k in FAR_FIRST:
+        for core in (1, 0):
             greet(z * NY + at_y(k), x * 2 + core)
     greet(zp * NY + y, tp)
     greet(zm * NY + y, tp)
@@ -88,7 +89,7 @@
     def y_send_sib():
         return copy(wpad.at[c], own_rows(c), y_ss, y_rs, fs, sib)
 
-    for k in range(1, NY):
+    for k in FAR_FIRST:
         y_send(k, 0).start()
     y_send_sib().start()
 
@@ -115,7 +116,7 @@
     for h in range(2):
         for way in range(2):
             c_own(h if way == 0 else 1 - h, way).start()
-    for k in range(1, NY):
+    for k in FAR_FIRST:
         y_send(k, 1).start()
     for h in range(2):
         c_own(h, 2).start()
@@ -265,7 +266,7 @@
                     sendy[bl, core] = own.reshape(NY, 3, 8, 128).astype(BF16)
                     sendy[bl, 1 - core] = other.reshape(NY, 3, 8, 128).astype(BF16)
             recvy[b, y] = sendy[bl, c, y]
-            for ky in range(1, NY):
+            for ky in FAR_FIRST:
                 for core in range(2):
                     piece(bl, ky, core).start()
             piece(bl, 0, 1 - c).start()

time: 62 us -> 60.3 us (0.973)
  Pallas kernels: 60 us -> 58.2 us
    pallas_call x1, Pallas kernels: 60 us -> 58.2 us  [local(): pl.pallas_call(kernel, out_shape=(pltpu.VMEM((toks, cols), BF16), pltpu.V...]
where the time goes in v5:
time: 60.3 us; the launch traced here: 60.1 us
  Pallas kernels  58.2 us (97%)
  local copies, waits for them, and re-layouts  1.27 us (2%)
  between operations  0.64 us (1%)
    pallas_call x1, Pallas kernels, local(): pl.pallas_call(kernel, out_shape=(pltpu.VMEM((toks, cols), BF16), pltpu.V...  58.2 us
    unnamed x2, local copies, waits for them, and re-layouts  1.27 us

profile of v5, /device:TPU:1, one launch (start us, length us, event | category | flops | bytes accessed | tf_op | source)
XLA Modules:
  0.0 60.1 jit_solution(9761737253782586733)
XLA Ops:
  0.6 58.2 %shard_map.68 = (bf16[640,128]{1,0:T(8,128)(2,1)S(1)}, f32[22,128]{1,0:T(8,128)S(1)}) custom-call(bf16[640,128]{1,0:T(8,128)(2,1)} %cot_hbm.1, bf16[640,128]{1,0:T(8,128)(2,1)} %inp_hbm.1, bf16[2112,640]{1,0:T(8,128)(2,1)} %bitcast.1, bf16[22,128]{1,0:T(8,128)(2,1)} %wu_hbm.1, bf16[22,128]{1,0:T(8,128)(2,1)} %wd_hbm.1), custom_call_target="tpu_custom_call" | custom-call | tf_op jit(solution)/shard_map/pallas_call | solution.py:423
  58.9 0.7 %copy.9 = bf16[640,128]{1,0:T(8,128)(2,1)} copy(bf16[640,128]{1,0:T(8,128)(2,1)S(1)} %get-tuple-element.2) | data formatting | bytes 327680
  59.5 0.6 copy.10

commit v6 on v5

--- a/solution.py
+++ b/solution.py
@@ -40,6 +40,16 @@
             device_id=(to_fs, to_tp), device_id_type=MESH,
         )
 
+    own_pre = pre_hbm.at[pl.ds(c * (half_z * hid), half_z * hid)]
+    loads = [
+        pltpu.make_async_copy(src, dst, load_sem.at[k])
+        for k, (src, dst) in enumerate(
+            ((wd_hbm, wd_ref), (wu_hbm, wu_ref), (cot_hbm, cot_ref), (inp_hbm, inp_ref), (own_pre, pre))
+        )
+    ]
+    for load in loads[:2]:
+        load.start()
+
     barrier = pltpu.get_barrier_semaphore()
 
     def greet(to_fs, to_tp):
@@ -58,14 +68,7 @@
         greet(fs, xl * 2 + core)
     greet(fs, sib)
 
-    own_pre = pre_hbm.at[pl.ds(c * (half_z * hid), half_z * hid)]
-    loads = [
-        pltpu.make_async_copy(src, dst, load_sem.at[k])
-        for k, (src, dst) in enumerate(
-            ((wd_hbm, wd_ref), (wu_hbm, wu_ref), (cot_hbm, cot_ref), (inp_hbm, inp_ref), (own_pre, pre))
-        )
-    ]
-    for load in loads:
+    for load in loads[2:]:
         load.start()
 
     keep = lax.broadcasted_iota(jnp.int32, (24, rows), 0) == lax.broadcasted_iota(jnp.int32, (24, rows), 1)

time: 60.3 us -> 60.3 us (level)
  no operation moved by 1% of the time
where the time goes in v6:
time: 60.3 us; the launch traced here: 60.1 us
  Pallas kernels  58.2 us (97%)
  local copies, waits for them, and re-layouts  1.27 us (2%)
  between operations  0.64 us (1%)
    pallas_call x1, Pallas kernels, local(): pl.pallas_call(kernel, out_shape=(pltpu.VMEM((toks, cols), BF16), pltpu.V...  58.2 us
    unnamed x2, local copies, waits for them, and re-layouts  1.27 us

profile of v6, /device:TPU:1, one launch (start us, length us, event | category | flops | bytes accessed | tf_op | source)
XLA Modules:
  0.0 60.1 jit_solution(1966925079863050166)
XLA Ops:
  0.6 58.2 %shard_map.68 = (bf16[640,128]{1,0:T(8,128)(2,1)S(1)}, f32[22,128]{1,0:T(8,128)S(1)}) custom-call(bf16[640,128]{1,0:T(8,128)(2,1)} %cot_hbm.1, bf16[640,128]{1,0:T(8,128)(2,1)} %inp_hbm.1, bf16[2112,640]{1,0:T(8,128)(2,1)} %bitcast.1, bf16[22,128]{1,0:T(8,128)(2,1)} %wu_hbm.1, bf16[22,128]{1,0:T(8,128)(2,1)} %wd_hbm.1), custom_call_target="tpu_custom_call" | custom-call | tf_op jit(solution)/shard_map/pallas_call | solution.py:426
  58.9 0.7 %copy.9 = bf16[640,128]{1,0:T(8,128)(2,1)} copy(bf16[640,128]{1,0:T(8,128)(2,1)S(1)} %get-tuple-element.2) | data formatting | bytes 327680
  59.5 0.6 copy.10
